TPU v7x, 1024 devices: a whole 8x8x8 slice. The times are simulated.
1024 devices in a mesh: dp: 8 (over x), kv: 64 (over z, y), tp: 2 (over core).
Axes of the slice: x: 8, y: 8, z: 8, core: 2. Of those that a mesh axis runs over, the one named last changes fastest.
Arguments:
- tokens: bfloat16 [128, 4096], P('dp', 'kv'), may hold values from -51 to 51
- norm_gain: float32 [4096], P('kv'), may hold values from 0.1 to 1.9
- w_query: bfloat16 [4096, 2048], P('kv', 'tp'), may hold values from -0.09375 to 0.09375
- lambda_head: float32 [16], P('tp'), may hold values from 0.3 to 0.8
- head_gain: float32 [128], replicated, may hold values from 0.1 to 1.9
- w_out: bfloat16 [2048, 4096], P('tp', 'kv'), may hold values from -0.125 to 0.125
- rotated_key_cache: bfloat16 [128, 16384, 128], P('dp', 'kv'), may hold values from -540 to 540, as said below
- value_cache: bfloat16 [128, 16384, 128], P('dp', 'kv'), may hold values from -6 to 6
- lengths: int32 [128], P('dp'), may hold values from 4096 to 16384
Outputs:
- mixed: bfloat16 [128, 4096], P('dp', ('kv', 'tp'))
Inputs may be any that keep to these rules, and one draw needn't show every extreme that they name: `rotated_key_cache`: keys have an order-one typical size. The new token is the last filled position, lengths - 1.
All inputs are finite; a program needn't handle non-finite values.
Results may differ from a plain program's by a relative error of at most 0.0112.
Values may be sent and summed in bfloat16 or wider, within the bound.
A program may use at most 32 MiB of HBM per device.

v0:
```python
import math

import jax
import jax.numpy as jnp
from jax import lax
from jax.sharding import PartitionSpec as P

D = 4096
HEAD_FEATURES = 64
VALUE_DIM = 128


EPS = 1e-05


def sent_to_all(x, axis):
    size = lax.axis_size(axis)
    return lax.all_to_all(jnp.broadcast_to(x[None], (size, *x.shape)), axis, 0, 0, tiled=True)


def of_everyone(x, axis):
    return sent_to_all(x, axis).sum(axis=0)


def taken_together(x, axis):
    return sent_to_all(x, axis).max(axis=0)


def split_up(x, dim, size):
    dims = x.shape
    parts = x.reshape(*dims[:dim], size, dims[dim] // size, *dims[dim + 1 :])
    return jnp.moveaxis(parts, dim, 0)


def sum_at_owner(x, axis, dim):
    size = lax.axis_size(axis)
    parts = lax.all_to_all(split_up(x, dim, size), axis, 0, 0, tiled=True)
    return jnp.sum(parts, axis=0)


def sent_together(arrays, axis, dim, along):
    widths = [math.prod(a.shape[along:]) for a in arrays]
    both = jnp.concatenate(
        [a.reshape(*a.shape[:along], w) for a, w in zip(arrays, widths)], axis=along
    )
    result = sum_at_owner(both, axis, dim)
    parts = jnp.split(result, [sum(widths[:k]) for k in range(1, len(widths))], axis=along)
    return tuple(
        (b.reshape(*result.shape[:along], *a.shape[along:]) for a, b in zip(arrays, parts))
    )


def laid_out(parts, dim):
    parts = jnp.moveaxis(parts, 0, dim)
    dims = parts.shape
    return parts.reshape(*dims[:dim], dims[dim] * dims[dim + 1], *dims[dim + 2 :])


def collect(x, axis, dim):
    return laid_out(sent_to_all(x, axis), dim)


def rotate_query(query, position):
    half_dim = query.shape[-1] // 2
    frequency = 1.0 / 10000.0 ** (jnp.arange(half_dim, dtype=jnp.float32) / half_dim)
    angles = position[:, None] * frequency[None, :]
    cosine_table = jnp.concatenate([jnp.cos(angles), jnp.cos(angles)], -1)[:, None, None, :]
    sine_table = jnp.concatenate([jnp.sin(angles), jnp.sin(angles)], -1)[:, None, None, :]
    first_half = query[..., :half_dim]
    second_half = query[..., half_dim:]
    turned = jnp.concatenate([-second_half, first_half], -1)
    return query * cosine_table + turned * sine_table


def finish(numerators, totals, lambdas, head_gain):
    averaged = numerators / totals[..., None]
    head_result = averaged[..., 0, :] - lambdas[..., None] * averaged[..., 1, :]
    factor = lax.rsqrt(jnp.mean(head_result * head_result, -1, keepdims=True) + EPS)
    return (head_result * factor * head_gain).astype(jnp.bfloat16)


def on_device(
    tokens,
    norm_gain,
    w_query,
    lambda_head,
    head_gain,
    w_out,
    rotated_key_cache,
    value_cache,
    lengths,
):
    seq_count = tokens.shape[0]
    head_count = lambda_head.shape[0]
    pos_count = rotated_key_cache.shape[1]
    widened = tokens.astype(jnp.float32)
    squares = jnp.sum(widened * widened, -1)
    scaled_in = (widened * norm_gain).astype(jnp.bfloat16)
    partial_query = jnp.dot(scaled_in, w_query, preferred_element_type=jnp.float32)
    squares = of_everyone(squares, "kv")
    raw_query = of_everyone(partial_query, "kv")
    scale_rows = lax.rsqrt(squares / D + EPS)
    shaped = (raw_query * scale_rows[:, None]).reshape(seq_count, head_count, 2, HEAD_FEATURES)
    query = rotate_query(shaped, (lengths - 1).astype(jnp.float32))
    keys = rotated_key_cache.reshape(seq_count, pos_count, 2, HEAD_FEATURES)
    score_rows = jnp.einsum(
        "bhmd,bpmd->bhmp",
        query,
        keys,
        preferred_element_type=jnp.float32,
        precision=lax.Precision.HIGHEST,
    ) * HEAD_FEATURES ** (-0.5)
    position_list = lax.axis_index("kv") * pos_count + jnp.arange(pos_count, dtype=jnp.int32)
    valid = (position_list[None, :] < lengths[:, None])[:, None, None, :]
    masked = jnp.where(valid, score_rows, -1e30)
    maxima = jnp.max(masked, -1)
    weights = jnp.where(valid, jnp.exp(masked - maxima[..., None]), 0.0)
    totals = jnp.sum(weights, -1)
    numerators = jnp.einsum(
        "bhmp,bpv->bhmv",
        weights.astype(jnp.bfloat16),
        value_cache,
        preferred_element_type=jnp.float32,
    )
    top = taken_together(maxima, "kv")
    factor = jnp.exp(maxima - top)
    row_count = seq_count * head_count
    numer_rows = (numerators * factor[..., None]).reshape(row_count, 2, VALUE_DIM)
    total_rows = (totals * factor).reshape(row_count, 2)
    numer_share, total_share = sent_together((numer_rows, total_rows), "kv", 0, 2)
    share_count = numer_share.shape[0]
    lambda_rows = lax.dynamic_slice_in_dim(
        jnp.tile(lambda_head, seq_count), lax.axis_index("kv") * share_count, share_count
    )
    normed_share = finish(numer_share, total_share, lambda_rows, head_gain)
    normed = collect(normed_share, "kv", 0).reshape(seq_count, head_count * VALUE_DIM)
    projected = jnp.dot(normed, w_out, preferred_element_type=jnp.float32)
    return sum_at_owner(projected, "tp", 1).astype(jnp.bfloat16)


def solution(mesh):
    in_specs = (
        P("dp", "kv"),
        P("kv"),
        P("kv", "tp"),
        P("tp"),
        P(),
        P("tp", "kv"),
        P("dp", "kv", None),
        P("dp", "kv", None),
        P("dp"),
    )
    out_specs = P("dp", ("kv", "tp"))
    return jax.shard_map(
        on_device, mesh=mesh, in_specs=in_specs, out_specs=out_specs, check_vma=False
    )
```

profile of v0, /device:TPU:1, one launch (start us, length us, event | category | flops | bytes accessed | tf_op | source)
XLA Modules:
  0.0 252.7 jit_solution(9304633693193514275)
XLA Ops:
  0.0 0.9 fusion.12
  0.9 0.6 broadcast_in_dim.31
  1.5 23.9 %all-to-all-start.1 = ((f32[64,1,16]{2,1,0:T(1,128)}), f32[64,1,16]{2,1,0:T(1,128)S(1)}, u32[]{:S(2)}, u32[]{:S(2)}) async-start(f32[64,1,16]{2,1,0:T(1,128)} %broadcast_in_dim.31), calls=%async_computation.1 | async-start | bytes 65536 | tf_op jit(solution)/shard_map/all_to_all | solution.py:18
  25.5 1.1 fusion.13
  26.5 9.8 %all-to-all-done.1 = f32[64,1,16]{2,1,0:T(1,128)S(1)} async-done(((f32[64,1,16]{2,1,0:T(1,128)}), f32[64,1,16]{2,1,0:T(1,128)S(1)}, u32[]{:S(2)}, u32[]{:S(2)}) %all-to-all-start.1) | async-done | bytes 4128 | tf_op jit(solution)/shard_map/all_to_all | solution.py:18
  36.3 2.5 broadcast_in_dim.30
  38.8 5.8 %all-to-all-start = ((f32[64,16,1024]{2,1,0:T(8,128)}), f32[64,16,1024]{2,1,0:T(8,128)}, u32[]{:S(2)}, u32[]{:S(2)}) async-start(f32[64,16,1024]{2,1,0:T(8,128)} %broadcast_in_dim.30), calls=%async_computation | async-start | bytes 8388608 | tf_op jit(solution)/shard_map/all_to_all | solution.py:18
  44.6 0.5 copy.64
  45.6 104.3 %all-to-all-done = f32[64,16,1024]{2,1,0:T(8,128)} async-done(((f32[64,16,1024]{2,1,0:T(8,128)}), f32[64,16,1024]{2,1,0:T(8,128)}, u32[]{:S(2)}, u32[]{:S(2)}) %all-to-all-start) | async-done | bytes 4194336 | tf_op jit(solution)/shard_map/all_to_all | solution.py:18
  149.9 2.4 reduce_sum.65
  152.5 0.2 slice_negate_fusion
  152.7 0.3 fusion.6
  153.0 0.6 fusion.21
  153.8 0.8 reshape.174
  154.6 40.2 %all-to-all-start.2 = ((f32[64,1,256]{2,1,0:T(1,128)}), f32[64,1,256]{2,1,0:T(1,128)S(1)}, u32[]{:S(2)}, u32[]{:S(2)}) async-start(f32[64,1,256]{2,1,0:T(1,128)} %reshape.174), calls=%async_computation.2 | async-start | bytes 131072 | tf_op jit(solution)/shard_map/all_to_all | solution.py:18
  194.8 0.2 fusion.3
  195.1 10.8 %all-to-all-done.2 = f32[64,1,256]{2,1,0:T(1,128)S(1)} async-done(((f32[64,1,256]{2,1,0:T(1,128)}), f32[64,1,256]{2,1,0:T(1,128)S(1)}, u32[]{:S(2)}, u32[]{:S(2)}) %all-to-all-start.2) | async-done | bytes 65568 | tf_op jit(solution)/shard_map/all_to_all | solution.py:18
  205.9 0.5 broadcast.121
  206.4 0.8 reduce.1
  207.2 0.2 reshape.175
  207.6 0.3 convolution_multiply_fusion.1
  208.0 0.2 mul.150
  208.4 0.7 copy.73
  209.1 4.6 %all-to-all-start.3 = ((f32[64,2,2,129]{3,1,2,0:T(2,128)}), f32[64,2,2,129]{3,1,2,0:T(2,128)S(1)}, u32[]{:S(2)}, u32[]{:S(2)}) async-start(f32[64,2,2,129]{3,1,2,0:T(2,128)} %copy.73), calls=%async_computation.3 | async-start | bytes 524288 | tf_op jit(solution)/shard_map/all_to_all | solution.py:37
  213.9 12.3 %all-to-all-done.3 = f32[64,2,2,129]{3,1,2,0:T(2,128)S(1)} async-done(((f32[64,2,2,129]{3,1,2,0:T(2,128)}), f32[64,2,2,129]{3,1,2,0:T(2,128)S(1)}, u32[]{:S(2)}, u32[]{:S(2)}) %all-to-all-start.3) | async-done | bytes 132128 | tf_op jit(solution)/shard_map/all_to_all | solution.py:37
  226.3 0.1 reduce_sum.70
  226.6 0.2 multiply_reduce_fusion
  226.9 14.7 %all_to_all.31 = bf16[64,2,128]{2,1,0:T(2,128)(2,1)S(1)} all-to-all(bf16[64,2,128]{2,1,0:T(2,128)(2,1)S(1)} %broadcast_in_dim.35), channel_id=1, replica_groups=mesh['dp'=8,'kv'=64,'tp'=2] {'kv'}, dimensions={0} | all-to-all | bytes 65536 | tf_op jit(solution)/shard_map/all_to_all | solution.py:18
  241.6 0.2 convolution_bitcast_fusion
  241.9 9.5 %all_to_all.32 = f32[2,1,512]{2,1,0:T(1,128)S(1)} all-to-all(f32[2,1,512]{2,1,0:T(1,128)S(1)} %reshape.176), channel_id=1, replica_groups=mesh['dp'=8,'kv'=64,'tp'=2] {'tp'}, dimensions={0} | all-to-all | bytes 8192 | tf_op jit(solution)/shard_map/all_to_all | solution.py:37
  251.3 0.7 reduce.2
  252.1 0.6 reduce_sum.72
  (43 shorter events, 1.8 us)
Async XLA Ops:
  0.0 207.6 %copy-start = (bf16[16,256,128]{2,1,0:T(8,128)(2,1)S(1)}, bf16[16,256,128]{2,1,0:T(8,128)(2,1)}, u32[]{:S(2)}) copy-start(bf16[16,256,128]{2,1,0:T(8,128)(2,1)} %param.16) | copy-start | bytes 3145732
  1.5 34.8 %all-to-all-start.1 = ((f32[64,1,16]{2,1,0:T(1,128)}), f32[64,1,16]{2,1,0:T(1,128)S(1)}, u32[]{:S(2)}, u32[]{:S(2)}) async-start(f32[64,1,16]{2,1,0:T(1,128)} %broadcast_in_dim.31), calls=%async_computation.1 | async-start | bytes 65536 | tf_op jit(solution)/shard_map/all_to_all | solution.py:18
  38.8 5.8 %copy-start.1 = (bf16[16,256,128]{2,1,0:T(8,128)(2,1)S(1)}, bf16[16,256,128]{2,1,0:T(8,128)(2,1)}, u32[]{:S(2)}) copy-start(bf16[16,256,128]{2,1,0:T(8,128)(2,1)} %param.15) | copy-start | bytes 3145732
  38.8 6.4 %copy-start.5 = (s32[16]{0:T(128)S(1)}, s32[16]{0:T(128)}, u32[]{:S(2)}) copy-start(s32[16]{0:T(128)} %param.17) | copy-start | bytes 196
  38.8 111.1 %all-to-all-start = ((f32[64,16,1024]{2,1,0:T(8,128)}), f32[64,16,1024]{2,1,0:T(8,128)}, u32[]{:S(2)}, u32[]{:S(2)}) async-start(f32[64,16,1024]{2,1,0:T(8,128)} %broadcast_in_dim.30), calls=%async_computation | async-start | bytes 8388608 | tf_op jit(solution)/shard_map/all_to_all | solution.py:18
  153.0 60.7 %copy-start.3 = (f32[8]{0:T(128)S(1)}, f32[8]{0:T(128)}, u32[]{:S(2)}) copy-start(f32[8]{0:T(128)} %param.12) | copy-start | bytes 100
  153.0 73.8 %copy-start.4 = (f32[128]{0:T(128)S(1)}, f32[128]{0:T(128)}, u32[]{:S(2)}) copy-start(f32[128]{0:T(128)} %param.13) | copy-start | bytes 1540
  153.0 88.5 %copy-start.2 = (bf16[1024,64]{0,1:T(8,128)(2,1)S(1)}, bf16[1024,64]{0,1:T(8,128)(2,1)}, u32[]{:S(2)}) copy-start(bf16[1024,64]{0,1:T(8,128)(2,1)} %param.14) | copy-start | bytes 393220
  154.6 51.3 %all-to-all-start.2 = ((f32[64,1,256]{2,1,0:T(1,128)}), f32[64,1,256]{2,1,0:T(1,128)S(1)}, u32[]{:S(2)}, u32[]{:S(2)}) async-start(f32[64,1,256]{2,1,0:T(1,128)} %reshape.174), calls=%async_computation.2 | async-start | bytes 131072 | tf_op jit(solution)/shard_map/all_to_all | solution.py:18
  209.1 17.1 %all-to-all-start.3 = ((f32[64,2,2,129]{3,1,2,0:T(2,128)}), f32[64,2,2,129]{3,1,2,0:T(2,128)S(1)}, u32[]{:S(2)}, u32[]{:S(2)}) async-start(f32[64,2,2,129]{3,1,2,0:T(2,128)} %copy.73), calls=%async_computation.3 | async-start | bytes 524288 | tf_op jit(solution)/shard_map/all_to_all | solution.py:37
where the time goes:
time: 253 us
  waiting for transfers between devices  137 us (54%)
  starting transfers between devices  74.5 us (29%)
  blocking collectives  24.2 us (10%)
  other arithmetic  7.21 us (3%)
  local copies, waits for them, and re-layouts  7.14 us (3%)
    all_to_all x3, waiting for transfers between devices, sent_to_all(): lax.all_to_all(jnp.broadcast_to(x[None], (size, *x.shape)), axis, 0, 0, t...  125 us
    all_to_all x3, starting transfers between devices, sent_to_all(): lax.all_to_all(jnp.broadcast_to(x[None], (size, *x.shape)), axis, 0, 0, t...  69.9 us
    all_to_all x1, blocking collectives, sent_to_all(): lax.all_to_all(jnp.broadcast_to(x[None], (size, *x.shape)), axis, 0, 0, t...  14.7 us
    all_to_all x1, waiting for transfers between devices, sum_at_owner(): parts = lax.all_to_all(split_up(x, dim, size), axis, 0, 0, tiled=True)  12.3 us
    all_to_all x1, blocking collectives, sum_at_owner(): parts = lax.all_to_all(split_up(x, dim, size), axis, 0, 0, tiled=True)  9.48 us
  transfers between devices with their start and end apart: 4, of which 4 were waited for; matrix products, arithmetic and copies ran while one was open for 1% of the time, Pallas kernels for 0%

commit v1 on v0

v1 whole, which is shorter than its diff:
```python
import functools

import jax
import jax.numpy as jnp
import numpy as np
from jax import lax
from jax.experimental import pallas as pl
from jax.experimental.pallas import tpu as pltpu
from jax.sharding import PartitionSpec as P

D = 4096
EPS = 1e-05
NEG = -1e30
N = 8
FAR_FIRST = (4, 3, 5, 2, 6, 1, 7)
NEAR_FIRST = (1, 7, 2, 6, 3, 5, 4)
MESH = pl.DeviceIdType.MESH
F32 = jnp.float32
BF16 = jnp.bfloat16


def kernel(
    tok_hbm, gain_hbm, wq_hbm, lam_hbm, hgain_hbm, wo_hbm, k_hbm, v_hbm, len_hbm, freq_hbm,
    out_ref,
    tok, gain, wq, lam, hgain, wo, kc, vc, lens, freq,
    qs, sqs, qr, sqr, zs, zsq, zr, zsqr, gs, gr,
    ns, ss, nr, sr, n2s, s2s, n2r, s2r, fs, fr, full, xs, xr,
    local_sem, send_sem, recv_sem, x_sem,
):
    kv = lax.axis_index("kv")
    tp = lax.axis_index("tp")
    y = lax.rem(kv, N)
    z = lax.div(kv, N)

    def y_id(d):
        return {"kv": z * N + lax.rem(y + d, N)}

    def z_id(d):
        return {"kv": lax.rem(z + d, N) * N + y}

    other = {"tp": 1 - tp}

    barrier = pltpu.get_barrier_semaphore()
    for d in FAR_FIRST:
        pl.semaphore_signal(barrier, inc=1, device_id=y_id(d), device_id_type=MESH)
        pl.semaphore_signal(barrier, inc=1, device_id=z_id(d), device_id_type=MESH)
    pl.semaphore_signal(barrier, inc=1, device_id=other, device_id_type=MESH)

    loads = []
    for i, (src, dst) in enumerate((
        (tok_hbm, tok), (gain_hbm, gain), (wq_hbm, wq), (len_hbm, lens), (freq_hbm, freq),
        (lam_hbm, lam), (hgain_hbm, hgain), (k_hbm, kc), (v_hbm, vc), (wo_hbm, wo),
    )):
        copy = pltpu.make_async_copy(src, dst, local_sem.at[i])
        copy.start()
        loads.append(copy)
    l_tok, l_gain, l_wq, l_len, l_freq, l_lam, l_hgain, l_k, l_v, l_wo = loads

    sends = []

    def send(phase, src, dst, d, ident):
        copy = pltpu.make_async_remote_copy(
            src_ref=src, dst_ref=dst.at[N - d],
            send_sem=send_sem.at[phase, N - d], recv_sem=recv_sem.at[phase, N - d],
            device_id=ident(d), device_id_type=MESH,
        )
        copy.start()
        sends.append(copy)

    def arrived(phase, src, dst, d):
        pltpu.make_async_remote_copy(
            src_ref=src, dst_ref=dst.at[d],
            send_sem=send_sem.at[phase, d], recv_sem=recv_sem.at[phase, d],
            device_id=y_id(0), device_id_type=MESH,
        ).wait_recv()

    l_tok.wait()
    l_gain.wait()
    x = tok[...].astype(F32)
    squares = jnp.broadcast_to(jnp.sum(x * x, -1, keepdims=True), (2 * N, 128))
    for j in range(N):
        sqs[j] = squares[2 * j : 2 * j + 2]
    scaled_in = (x * gain[...]).astype(BF16)
    l_wq.wait()
    partial = jnp.dot(scaled_in, wq[...], preferred_element_type=F32)
    for h in range(8):
        qs[pl.ds(h, 16, stride=8), :] = partial[:, 128 * h : 128 * h + 128]

    def mine(ref, rows):
        return ref[pl.ds(pl.multiple_of(y * rows, rows), rows), :]

    pl.semaphore_wait(barrier, 2 * (N - 1) + 1)
    for d in FAR_FIRST:
        yp = lax.rem(y + d, N)
        send(0, qs.at[pl.ds(pl.multiple_of(yp * 16, 16), 16), :], qr, d, y_id)
        send(1, sqs.at[yp], sqr, d, y_id)

    l_len.wait()
    l_freq.wait()
    lane = lax.broadcasted_iota(jnp.int32, (8, 128), 1)
    tables = []
    for b2 in range(2):
        position = (lens[2 * y + b2] - 1).astype(F32)
        angles = position * jnp.broadcast_to(freq[...], (8, 128))
        tables.append((jnp.cos(angles), jnp.sin(angles)))

    total_q = mine(qs, 16)
    total_sq = sqs[y]
    for d in NEAR_FIRST:
        arrived(0, zs, qr, d)
        total_q = total_q + qr[d]
        arrived(1, zsq, sqr, d)
        total_sq = total_sq + sqr[d]
    zs[...] = total_q
    zsq[...] = total_sq
    for d in FAR_FIRST:
        send(2, zs, zr, d, z_id)
        send(3, zsq, zsqr, d, z_id)
    for d in NEAR_FIRST:
        arrived(2, zs, zr, d)
        total_q = total_q + zr[d]
        arrived(3, zsq, zsqr, d)
        total_sq = total_sq + zsqr[d]
    scale = lax.rsqrt(total_sq / D + EPS)
    own = []
    for b2 in range(2):
        q = total_q[8 * b2 : 8 * b2 + 8] * scale[b2 : b2 + 1]
        turned = jnp.where((lane & 32) == 0, -pltpu.roll(q, 96, 1), pltpu.roll(q, 32, 1))
        cosine, sine = tables[b2]
        q = (q * cosine + turned * sine) * 0.125
        gs[8 * b2 : 8 * b2 + 8, :] = q
        own.append(q)
    for d in FAR_FIRST:
        send(4, gs, gr, d, y_id)

    l_k.wait()
    l_v.wait()
    group = lane // 16
    positions = kv * 256 + lax.broadcasted_iota(jnp.int32, (16, 256), 1)

    def attend(d, queries):
        j = lax.rem(y + d, N)
        stats = jnp.zeros((8, 128), F32)
        for b2 in range(2):
            b = 2 * j + b2
            q = queries[b2]
            rows = jnp.concatenate([jnp.where(lane < 64, q, 0.0), jnp.where(lane < 64, 0.0, q)], 0)
            high = rows.astype(BF16)
            low = (rows - high.astype(F32)).astype(BF16)
            scores = lax.dot_general(
                jnp.concatenate([high, low], 0), kc[b], (((1,), (1,)), ((), ())),
                preferred_element_type=F32,
            )
            scores = scores[:16] + scores[16:]
            valid = positions < lens[b]
            scores = jnp.where(valid, scores, NEG)
            top = jnp.max(scores, -1, keepdims=True)
            weights = jnp.where(valid, jnp.exp(scores - top), 0.0)
            totals = jnp.sum(weights, -1, keepdims=True)
            numer = jnp.dot(weights.astype(BF16), vc[b], preferred_element_type=F32)
            ns[d, 16 * b2 : 16 * b2 + 16, :] = numer.astype(BF16)
            for m in range(2):
                k = 2 * b2 + m
                stats = jnp.where(group == k, top[8 * m : 8 * m + 8], stats)
                stats = jnp.where(group == 4 + k, totals[8 * m : 8 * m + 8], stats)
        ss[d] = stats

    attend(0, own)
    for d in NEAR_FIRST:
        arrived(4, gs, gr, d)
        attend(d, (gr[d, 0:8, :], gr[d, 8:16, :]))
        send(6, ss.at[d], sr, d, y_id)
        send(5, ns.at[d], nr, d, y_id)

    def combined(phase, stats, numer, stat_src, stat_slots, numer_src, numer_slots):
        stat = [stats]
        for d in NEAR_FIRST:
            arrived(phase + 1, stat_src, stat_slots, d)
            stat.append(stat_slots[d])
        top = functools.reduce(jnp.maximum, stat)
        factors = [jnp.exp(s - top) for s in stat]
        total = sum(pltpu.roll(f, 64, 1) * s for f, s in zip(factors, stat))
        sums = [factors[0][:, 16 * k : 16 * k + 1] * numer[8 * k : 8 * k + 8] for k in range(4)]
        for i, d in enumerate(NEAR_FIRST):
            arrived(phase, numer_src, numer_slots, d)
            block = numer_slots[d].astype(F32)
            for k in range(4):
                sums[k] = sums[k] + factors[i + 1][:, 16 * k : 16 * k + 1] * block[8 * k : 8 * k + 8]
        return jnp.where(lane < 64, top, total), sums

    stats, sums = combined(5, ss[0], ns[0].astype(F32), s2s, sr, n2s, nr)
    numer = jnp.concatenate(sums, 0)
    s2s[...] = stats
    n2s[...] = numer.astype(BF16)
    for d in FAR_FIRST:
        send(8, s2s, s2r, d, z_id)
        send(7, n2s, n2r, d, z_id)
    l_lam.wait()
    l_hgain.wait()
    row = lax.broadcasted_iota(jnp.int32, (8, 128), 0)
    lambdas = jnp.zeros((8, 128), F32)
    for h in range(8):
        lambdas = jnp.where(row == h, lam[h], lambdas)
    stats, sums = combined(7, stats, numer, s2s, s2r, n2s, n2r)
    normed = []
    for b2 in range(2):
        first, second = (
            sums[k] / stats[:, 64 + 16 * k : 65 + 16 * k] for k in (2 * b2, 2 * b2 + 1)
        )
        head = first - lambdas * second
        factor = lax.rsqrt(jnp.mean(head * head, -1, keepdims=True) + EPS)
        normed.append(head * factor * hgain[...])
    normed = jnp.concatenate(normed, 0).astype(BF16)
    fs[...] = normed
    for d in FAR_FIRST:
        send(9, fs, fr, d, y_id)
    full[pl.ds(pl.multiple_of(y * 16, 16), 16), :] = normed.astype(F32)
    l_wo.wait()
    for d in NEAR_FIRST:
        arrived(9, fs, fr, d)
        full[pl.ds(pl.multiple_of(lax.rem(y + d, N) * 16, 16), 16), :] = fr[d].astype(F32)
    flat = jnp.concatenate([full[pl.ds(h, 16, stride=8), :] for h in range(8)], 1).astype(BF16)
    mixed = lax.dot_general(flat, wo[...], (((1,), (1,)), ((), ())), preferred_element_type=F32)
    low, high = mixed[:, :32], mixed[:, 32:]
    xs[...] = jnp.where(tp == 0, high, low)
    swap = pltpu.make_async_remote_copy(
        src_ref=xs, dst_ref=xr, send_sem=x_sem.at[0], recv_sem=x_sem.at[1],
        device_id=other, device_id_type=MESH,
    )
    swap.start()
    kept = jnp.where(tp == 0, low, high)
    swap.wait()
    out_ref[...] = (kept + xr[...]).astype(BF16)
    for copy in sends:
        copy.wait_send()


def on_device(tokens, norm_gain, w_query, lambda_head, head_gain, w_out, keys, values, lengths):
    frequency = 1.0 / 10000.0 ** (np.arange(32, dtype=np.float32) / np.float32(32))
    freq = jnp.asarray(np.tile(frequency.astype(np.float32), 4)[None, :])
    operands = (
        tokens, norm_gain[None, :], w_query, lambda_head, head_gain[None, :], w_out.T, keys, values,
        lengths, freq,
    )
    vmem = pltpu.VMEM
    local = [vmem(a.shape, a.dtype) for a in operands]
    local[3] = pltpu.SMEM((8,), F32)
    local[8] = pltpu.SMEM((16,), jnp.int32)
    scratch = local + [
        vmem((128, 128), F32), vmem((N, 2, 128), F32), vmem((N, 16, 128), F32), vmem((N, 2, 128), F32),
        vmem((16, 128), F32), vmem((2, 128), F32), vmem((N, 16, 128), F32), vmem((N, 2, 128), F32),
        vmem((16, 128), F32), vmem((N, 16, 128), F32),
        vmem((N, 32, 128), BF16), vmem((N, 8, 128), F32), vmem((N, 32, 128), BF16), vmem((N, 8, 128), F32),
        vmem((32, 128), BF16), vmem((8, 128), F32), vmem((N, 32, 128), BF16), vmem((N, 8, 128), F32),
        vmem((16, 128), BF16), vmem((N, 16, 128), BF16), vmem((128, 128), F32),
        vmem((16, 32), F32), vmem((16, 32), F32),
        pltpu.SemaphoreType.DMA((10,)), pltpu.SemaphoreType.DMA((10, N)),
        pltpu.SemaphoreType.DMA((10, N)), pltpu.SemaphoreType.DMA((2,)),
    ]
    return pl.pallas_call(
        kernel,
        name="step",
        out_shape=jax.ShapeDtypeStruct((16, 32), BF16),
        in_specs=[pl.BlockSpec(memory_space=pl.ANY)] * len(operands),
        out_specs=pl.BlockSpec(memory_space=pltpu.VMEM),
        scratch_shapes=scratch,
        compiler_params=pltpu.CompilerParams(collective_id=0, has_side_effects=True),
    )(*operands)


def solution(mesh):
    in_specs = (
        P("dp", "kv"),
        P("kv"),
        P("kv", "tp"),
        P("tp"),
        P(),
        P("tp", "kv"),
        P("dp", "kv", None),
        P("dp", "kv", None),
        P("dp"),
    )
    return jax.shard_map(
        on_device, mesh=mesh, in_specs=in_specs, out_specs=P("dp", ("kv", "tp")), check_vma=False
    )
```

time: 253 us -> 58.3 us (0.23)
  waiting for transfers between devices: 137 us -> 0 us
  starting transfers between devices: 74.5 us -> 0 us
  Pallas kernels: 0 us -> 56.8 us
  blocking collectives: 24.2 us -> 0 us
  other arithmetic: 7.21 us -> 0 us
  local copies, waits for them, and re-layouts: 7.14 us -> 1.28 us
    all_to_all x4 -> x0, waiting for transfers between devices: 137 us -> none  [the longest x3 125 us: sent_to_all(): lax.all_to_all(jnp.broadcast_to(x[None], (size, *x.shape)), axis, 0, 0, t...]
    all_to_all x4 -> x0, starting transfers between devices: 74.5 us -> none  [the longest x3 69.9 us: sent_to_all(): lax.all_to_all(jnp.broadcast_to(x[None], (size, *x.shape)), axis, 0, 0, t...]
    pallas_call x0 -> x1, Pallas kernels: none -> 56.8 us  [on_device(): pl.pallas_call(kernel, name='step', out_shape=jax.ShapeDtypeStruct((16, 3...]
    all_to_all x2 -> x0, blocking collectives: 24.2 us -> none  [the longest x1 14.7 us: sent_to_all(): lax.all_to_all(jnp.broadcast_to(x[None], (size, *x.shape)), axis, 0, 0, t...]
    reduce_sum x7 -> x0, other arithmetic: 4.52 us -> none  [the longest x2 2.5 us: of_everyone(): return sent_to_all(x, axis).sum(axis=0)]
    broadcast_in_dim x3 -> x0, local copies, waits for them, and re-layouts: 3.14 us -> none  [sent_to_all(): jnp.broadcast_to(x[None], (size, *x.shape))]
  transfers between devices with their start and end apart: 4 -> 0, of which waited for: 4 -> 0; matrix products, arithmetic and copies ran while one was open for 1% -> 0% of each run, Pallas kernels for 0% -> 0%
where the time goes in v1:
time: 58.3 us; the launch traced here: 58.1 us
  Pallas kernels  56.8 us (97%)
  local copies, waits for them, and re-layouts  1.28 us (2%)
    pallas_call x1, Pallas kernels, on_device(): pl.pallas_call(kernel, name='step', out_shape=jax.ShapeDtypeStruct((16, 3...  56.8 us
    unnamed x1, local copies, waits for them, and re-layouts  1.28 us

profile of v1, /device:TPU:1, one launch (start us, length us, event | category | flops | bytes accessed | tf_op | source)
XLA Modules:
  0.0 58.1 jit_solution(5198745895977067026)
XLA Ops:
  0.0 56.8 %step.1 = bf16[16,32]{1,0:T(8,128)(2,1)} custom-call(bf16[16,64]{1,0:T(8,128)(2,1)} %tok_hbm.1, f32[1,64]{1,0:T(1,128)} %bitcast.4, bf16[64,1024]{1,0:T(8,128)(2,1)} %wq_hbm.1, f32[8]{0:T(128)} %lam_hbm.1, f32[1,128]{1,0:T(1,128)} %bitcast.5, bf16[64,1024]{1,0:T(8,128)(2,1)} %bitcast.3, bf16[16,256,128]{2,1,0:T(8,128)(2,1)} %k_hbm.1, ...), custom_call_target="tpu_custom_call" | custom-call | tf_op jit(solution)/shard_map/step/pallas_call | solution.py:260
  56.8 1.3 %copy.12 = bf16[16,32]{1,0:T(8,128)(2,1)} copy(bf16[16,32]{1,0:T(8,128)(2,1)} %step.1) | data formatting | bytes 2048

commit v2 on v1

v2 whole, which is shorter than its diff:
```python
import functools

import jax
import jax.numpy as jnp
import numpy as np
from jax import lax
from jax.experimental import pallas as pl
from jax.experimental.pallas import tpu as pltpu
from jax.sharding import PartitionSpec as P

D = 4096
EPS = 1e-05
NEG = -1e30
N = 8
FAR_FIRST = (4, 3, 5, 2, 6, 1, 7)
NEAR_FIRST = (1, 7, 2, 6, 3, 5, 4)
MESH = pl.DeviceIdType.MESH
F32 = jnp.float32
BF16 = jnp.bfloat16


def kernel(
    tok_hbm, gain_hbm, wq_hbm, lam_hbm, hgain_hbm, wo_hbm, k_hbm, v_hbm, len_hbm, freq_hbm,
    out_ref,
    tok, gain, wq, lam, hgain, wo, kc, vc, lens, freq,
    qs, sqs, qr, sqr, zs, zsq, zr, zsqr, gs, gr,
    ns, ss, nr, sr, n2s, s2s, n2r, s2r, fs, fr, full,
    local_sem, send_sem, recv_sem, q_sem, wo_sem,
):
    kv = lax.axis_index("kv")
    tp = lax.axis_index("tp")
    y = lax.rem(kv, N)
    z = lax.div(kv, N)

    def y_id(d):
        return {"kv": z * N + lax.rem(y + d, N), "tp": 1}

    def z_id(d):
        return {"kv": lax.rem(z + d, N) * N + y, "tp": 1}

    def z_id0(d):
        return {"kv": lax.rem(z + d, N) * N + y, "tp": 0}

    barrier = pltpu.get_barrier_semaphore()

    def greet(ident):
        pl.semaphore_signal(barrier, inc=1, device_id=ident, device_id_type=MESH)

    for d in FAR_FIRST:
        greet(z_id(d))

    @pl.when(tp == 1)
    def _():
        for d in FAR_FIRST:
            greet(y_id(d))
        for d in (*FAR_FIRST, 0):
            greet(z_id0(d))

    @pl.when(tp == 0)
    def _():
        greet(z_id(0))

    def load(i, src, dst):
        return pltpu.make_async_copy(src, dst, local_sem.at[i])

    l_tok = load(0, tok_hbm, tok)
    l_gain = load(1, gain_hbm, gain)
    l_wq = load(2, wq_hbm, wq)
    l_wo = load(3, wo_hbm.at[pl.ds(pl.multiple_of(tp * 32, 32), 32), :], wo.at[tp])
    l_len = load(4, len_hbm, lens)
    l_freq = load(5, freq_hbm, freq)
    l_lam = load(6, lam_hbm, lam.at[tp])
    l_hgain = load(7, hgain_hbm, hgain)
    l_k = load(8, k_hbm, kc)
    l_v = load(9, v_hbm, vc)
    for copy in (l_tok, l_gain, l_wq, l_lam):
        copy.start()

    @pl.when(tp == 1)
    def _():
        for copy in (l_len, l_freq, l_hgain, l_k, l_v):
            copy.start()

    l_wo.start()

    def sent(phase, src, dst, d, ident):
        return pltpu.make_async_remote_copy(
            src_ref=src, dst_ref=dst.at[(N - d) % N],
            send_sem=send_sem.at[phase, d], recv_sem=recv_sem.at[phase, (N - d) % N],
            device_id=ident(d), device_id_type=MESH,
        )

    def arrived(phase, src, dst, d):
        pltpu.make_async_remote_copy(
            src_ref=src, dst_ref=dst.at[d],
            send_sem=send_sem.at[phase, d], recv_sem=recv_sem.at[phase, d],
            device_id=z_id0(0), device_id_type=MESH,
        ).wait_recv()

    l_tok.wait()
    l_gain.wait()
    x = tok[...].astype(F32)
    squares = jnp.broadcast_to(jnp.sum(x * x, -1, keepdims=True), (2 * N, 128))
    for j in range(N):
        sqs[j] = squares[2 * j : 2 * j + 2]
    scaled_in = (x * gain[...]).astype(BF16)
    l_wq.wait()
    partial = jnp.dot(scaled_in, wq[...], preferred_element_type=F32)
    for h in range(8):
        qs[pl.ds(h, 16, stride=8), :] = partial[:, 128 * h : 128 * h + 128]

    def query_copy(d):
        zp = lax.rem(z + d, N)
        slot = (N - d) % N
        return pltpu.make_async_remote_copy(
            src_ref=qs.at[pl.ds(pl.multiple_of(zp * 16, 16), 16), :], dst_ref=qr.at[tp, slot],
            send_sem=send_sem.at[0, d], recv_sem=q_sem.at[tp, slot],
            device_id=z_id(d), device_id_type=MESH,
        )

    def square_copy(d):
        return sent(1, sqs.at[lax.rem(z + d, N)], sqr, d, z_id)

    swap_wo = pltpu.make_async_remote_copy(
        src_ref=wo_hbm.at[pl.ds(pl.multiple_of((1 - tp) * 32, 32), 32), :], dst_ref=wo.at[tp],
        send_sem=wo_sem.at[0], recv_sem=wo_sem.at[1],
        device_id={"tp": 1 - tp}, device_id_type=MESH,
    )
    swap_lam = pltpu.make_async_remote_copy(
        src_ref=lam_hbm, dst_ref=lam.at[tp], send_sem=wo_sem.at[2], recv_sem=wo_sem.at[3],
        device_id={"tp": 1 - tp}, device_id_type=MESH,
    )

    @pl.when(tp == 0)
    def _():
        pl.semaphore_wait(barrier, N)

    @pl.when(tp == 1)
    def _():
        pl.semaphore_wait(barrier, 3 * N - 2)

    for d in FAR_FIRST:
        query_copy(d).start()

    @pl.when(tp == 0)
    def _():
        query_copy(0).start()

    @pl.when(tp == 1)
    def _():
        for d in FAR_FIRST:
            square_copy(d).start()

    swap_lam.start()
    swap_wo.start()

    def q_arrived(t, d):
        pltpu.make_async_remote_copy(
            src_ref=gs.at[t], dst_ref=qr.at[t, d],
            send_sem=send_sem.at[0, d], recv_sem=q_sem.at[t, d],
            device_id=z_id0(0), device_id_type=MESH,
        ).wait_recv()

    def exchanges():
        yield [sent(2, zs, zr, d, y_id) for d in FAR_FIRST]
        yield [sent(3, zsq, zsqr, d, y_id) for d in FAR_FIRST]
        yield [sent(4, gs, gr, d, z_id) for d in FAR_FIRST]
        yield [sent(6, ss.at[d], sr, d, z_id) for d in FAR_FIRST]
        yield [sent(5, ns.at[d], nr, d, z_id) for d in FAR_FIRST]
        yield [sent(8, s2s, s2r, d, y_id) for d in FAR_FIRST]
        yield [sent(7, n2s, n2r, d, y_id) for d in FAR_FIRST]

    @pl.when(tp == 1)
    def _():
        l_len.wait()
        l_freq.wait()
        lane = lax.broadcasted_iota(jnp.int32, (8, 128), 1)
        tables = []
        for b2 in range(2):
            position = (lens[2 * z + b2] - 1).astype(F32)
            angles = position * jnp.broadcast_to(freq[...], (8, 128))
            tables.append((jnp.cos(angles), jnp.sin(angles)))

        total_q = [None, qs[pl.ds(pl.multiple_of(z * 16, 16), 16), :]]
        total_sq = sqs[z]
        for d in NEAR_FIRST:
            q_arrived(1, d)
            total_q[1] = total_q[1] + qr[1, d]
            arrived(1, zsq, sqr, d)
            total_sq = total_sq + sqr[d]
        q_arrived(0, 0)
        total_q[0] = qr[0, 0]
        for d in NEAR_FIRST:
            q_arrived(0, d)
            total_q[0] = total_q[0] + qr[0, d]
        for t in range(2):
            zs[t] = total_q[t]
        zsq[...] = total_sq
        for d in FAR_FIRST:
            sent(2, zs, zr, d, y_id).start()
            sent(3, zsq, zsqr, d, y_id).start()
        for d in NEAR_FIRST:
            arrived(2, zs, zr, d)
            for t in range(2):
                total_q[t] = total_q[t] + zr[d, t]
            arrived(3, zsq, zsqr, d)
            total_sq = total_sq + zsqr[d]
        scale = lax.rsqrt(total_sq / D + EPS)
        own = []
        for b2 in range(2):
            cosine, sine = tables[b2]
            for t in range(2):
                q = total_q[t][8 * b2 : 8 * b2 + 8] * scale[b2 : b2 + 1]
                turned = jnp.where((lane & 32) == 0, -pltpu.roll(q, 96, 1), pltpu.roll(q, 32, 1))
                q = (q * cosine + turned * sine) * 0.125
                gs[t, 8 * b2 : 8 * b2 + 8, :] = q
                own.append(q)
        for d in FAR_FIRST:
            sent(4, gs, gr, d, z_id).start()

        l_k.wait()
        l_v.wait()
        group = lane // 8
        positions = kv * 256 + lax.broadcasted_iota(jnp.int32, (32, 256), 1)

        def attend(d, queries):
            j = lax.rem(z + d, N)
            stats = jnp.zeros((8, 128), F32)
            for b2 in range(2):
                b = 2 * j + b2
                q = queries[2 * b2 : 2 * b2 + 2]
                rows = jnp.concatenate(
                    [jnp.where(lane < 64, part, 0.0) for part in q]
                    + [jnp.where(lane < 64, 0.0, part) for part in q], 0
                )
                high = rows.astype(BF16)
                low = (rows - high.astype(F32)).astype(BF16)
                scores = lax.dot_general(
                    jnp.concatenate([high, low], 0), kc[b], (((1,), (1,)), ((), ())),
                    preferred_element_type=F32,
                )
                scores = scores[:32] + scores[32:]
                valid = positions < lens[b]
                scores = jnp.where(valid, scores, NEG)
                top = jnp.max(scores, -1, keepdims=True)
                weights = jnp.where(valid, jnp.exp(scores - top), 0.0)
                totals = jnp.sum(weights, -1, keepdims=True)
                numer = jnp.dot(weights.astype(BF16), vc[b], preferred_element_type=F32)
                ns[d, 32 * b2 : 32 * b2 + 32, :] = numer.astype(BF16)
                for i in range(4):
                    k = 4 * b2 + i
                    stats = jnp.where(group == k, top[8 * i : 8 * i + 8], stats)
                    stats = jnp.where(group == 8 + k, totals[8 * i : 8 * i + 8], stats)
            ss[d] = stats

        attend(0, own)
        for d in NEAR_FIRST:
            arrived(4, gs, gr, d)
            attend(d, [gr[d, t, 8 * b2 : 8 * b2 + 8, :] for b2 in range(2) for t in range(2)])
            sent(6, ss.at[d], sr, d, z_id).start()
            sent(5, ns.at[d], nr, d, z_id).start()

        def combined(phase, stats, numer, stat_src, stat_slots, numer_src, numer_slots):
            stat = [stats]
            for d in NEAR_FIRST:
                arrived(phase + 1, stat_src, stat_slots, d)
                stat.append(stat_slots[d])
            top = functools.reduce(jnp.maximum, stat)
            factors = [jnp.exp(s - top) for s in stat]
            total = sum(pltpu.roll(f, 64, 1) * s for f, s in zip(factors, stat))
            sums = [factors[0][:, 8 * k : 8 * k + 1] * numer[8 * k : 8 * k + 8] for k in range(8)]
            for i, d in enumerate(NEAR_FIRST):
                arrived(phase, numer_src, numer_slots, d)
                block = numer_slots[d].astype(F32)
                for k in range(8):
                    sums[k] = sums[k] + factors[i + 1][:, 8 * k : 8 * k + 1] * block[8 * k : 8 * k + 8]
            return jnp.where(lane < 64, top, total), sums

        stats, sums = combined(5, ss[0], ns[0].astype(F32), s2s, sr, n2s, nr)
        numer = jnp.concatenate(sums, 0)
        s2s[...] = stats
        n2s[...] = numer.astype(BF16)
        for d in FAR_FIRST:
            sent(8, s2s, s2r, d, y_id).start()
            sent(7, n2s, n2r, d, y_id).start()
        l_hgain.wait()
        l_lam.wait()
        swap_lam.wait()
        diagonal = lax.broadcasted_iota(jnp.int32, (8, 8), 0) == lax.broadcasted_iota(jnp.int32, (8, 8), 1)
        lambdas = [
            jnp.sum(jnp.where(diagonal, jnp.broadcast_to(lam[t], (8, 8)), 0.0), -1, keepdims=True)
            for t in range(2)
        ]
        stats, sums = combined(7, stats, numer, s2s, s2r, n2s, n2r)
        normed = []
        for b2 in range(2):
            for t in range(2):
                first, second = (
                    sums[k] / stats[:, 64 + 8 * k : 65 + 8 * k] for k in (4 * b2 + t, 4 * b2 + 2 + t)
                )
                head = first - lambdas[t] * second
                factor = lax.rsqrt(jnp.mean(head * head, -1, keepdims=True) + EPS)
                normed.append(head * factor * hgain[...])
        normed = jnp.concatenate(normed, 0).astype(BF16)
        fs[...] = normed
        sent(10, fs, fr, 0, z_id0).start()
        for d in FAR_FIRST:
            sent(10, fs, fr, d, z_id0).start()
            sent(9, fs, fr, d, z_id).start()
        full[pl.ds(pl.multiple_of(z * 32, 32), 32), :] = normed.astype(F32)

    def gathered(phase, d):
        arrived(phase, fs, fr, d)
        full[pl.ds(pl.multiple_of(lax.rem(z + d, N) * 32, 32), 32), :] = fr[d].astype(F32)

    l_wo.wait()
    swap_wo.wait()

    @pl.when(tp == 1)
    def _():
        for d in NEAR_FIRST:
            gathered(9, d)

    @pl.when(tp == 0)
    def _():
        l_lam.wait()
        swap_lam.wait()
        for d in (0, *NEAR_FIRST):
            gathered(10, d)

    mixed = jnp.zeros((16, 32), F32)
    for t in range(2):
        flat = jnp.concatenate([full[pl.ds(8 * t + h, 16, stride=16), :] for h in range(8)], 1)
        mixed = mixed + lax.dot_general(
            flat.astype(BF16), wo[t], (((1,), (1,)), ((), ())), preferred_element_type=F32
        )
    out_ref[...] = mixed.astype(BF16)

    for d in FAR_FIRST:
        query_copy(d).wait_send()

    @pl.when(tp == 0)
    def _():
        query_copy(0).wait_send()

    @pl.when(tp == 1)
    def _():
        for d in FAR_FIRST:
            square_copy(d).wait_send()
        for copies in exchanges():
            for copy in copies:
                copy.wait_send()
        sent(10, fs, fr, 0, z_id0).wait_send()
        for d in FAR_FIRST:
            sent(10, fs, fr, d, z_id0).wait_send()
            sent(9, fs, fr, d, z_id).wait_send()


def on_device(tokens, norm_gain, w_query, lambda_head, head_gain, w_out, keys, values, lengths):
    frequency = 1.0 / 10000.0 ** (np.arange(32, dtype=np.float32) / np.float32(32))
    freq = jnp.asarray(np.tile(frequency.astype(np.float32), 4)[None, :])
    operands = (
        tokens, norm_gain[None, :], w_query, lambda_head[None, :], head_gain[None, :], w_out.T, keys, values,
        lengths, freq,
    )
    vmem = pltpu.VMEM
    local = [vmem(a.shape, a.dtype) for a in operands]
    local[3] = vmem((2, 1, 8), F32)
    local[5] = vmem((2, 32, 1024), BF16)
    local[8] = pltpu.SMEM((16,), jnp.int32)
    scratch = local + [
        vmem((128, 128), F32), vmem((N, 2, 128), F32), vmem((2, N, 16, 128), F32), vmem((N, 2, 128), F32),
        vmem((2, 16, 128), F32), vmem((2, 128), F32), vmem((N, 2, 16, 128), F32), vmem((N, 2, 128), F32),
        vmem((2, 16, 128), F32), vmem((N, 2, 16, 128), F32),
        vmem((N, 64, 128), BF16), vmem((N, 8, 128), F32), vmem((N, 64, 128), BF16), vmem((N, 8, 128), F32),
        vmem((64, 128), BF16), vmem((8, 128), F32), vmem((N, 64, 128), BF16), vmem((N, 8, 128), F32),
        vmem((32, 128), BF16), vmem((N, 32, 128), BF16), vmem((256, 128), F32),
        pltpu.SemaphoreType.DMA((10,)), pltpu.SemaphoreType.DMA((11, N)),
        pltpu.SemaphoreType.DMA((11, N)), pltpu.SemaphoreType.DMA((2, N)), pltpu.SemaphoreType.DMA((4,)),
    ]
    return pl.pallas_call(
        kernel,
        name="step",
        out_shape=jax.ShapeDtypeStruct((16, 32), BF16),
        in_specs=[pl.BlockSpec(memory_space=pl.ANY)] * len(operands),
        out_specs=pl.BlockSpec(memory_space=pltpu.VMEM),
        scratch_shapes=scratch,
        compiler_params=pltpu.CompilerParams(collective_id=0, has_side_effects=True),
    )(*operands)


def solution(mesh):
    in_specs = (
        P("dp", "kv"),
        P("kv"),
        P("kv", "tp"),
        P("tp"),
        P(),
        P("tp", "kv"),
        P("dp", "kv", None),
        P("dp", "kv", None),
        P("dp"),
    )
    return jax.shard_map(
        on_device, mesh=mesh, in_specs=in_specs, out_specs=P("dp", ("kv", "tp")), check_vma=False
    )
```

time: 58.3 us -> 55.1 us (0.945)
  Pallas kernels: 56.8 us -> 53.6 us
    pallas_call x1, Pallas kernels: 56.8 us -> 53.6 us  [on_device(): pl.pallas_call(kernel, name='step', out_shape=jax.ShapeDtypeStruct((16, 3...]
where the time goes in v2:
time: 55.1 us; the launch traced here: 54.9 us
  Pallas kernels  53.6 us (97%)
  local copies, waits for them, and re-layouts  1.28 us (2%)
    pallas_call x1, Pallas kernels, on_device(): pl.pallas_call(kernel, name='step', out_shape=jax.ShapeDtypeStruct((16, 3...  53.6 us
    unnamed x1, local copies, waits for them, and re-layouts  1.28 us

profile of v2, /device:TPU:1, one launch (start us, length us, event | category | flops | bytes accessed | tf_op | source)
XLA Modules:
  0.0 54.9 jit_solution(9344644622092546885)
XLA Ops:
  0.0 53.6 %step.1 = bf16[16,32]{1,0:T(8,128)(2,1)} custom-call(bf16[16,64]{1,0:T(8,128)(2,1)} %tok_hbm.1, f32[1,64]{1,0:T(1,128)} %bitcast.5, bf16[64,1024]{1,0:T(8,128)(2,1)} %wq_hbm.1, f32[1,8]{1,0:T(1,128)} %bitcast.6, f32[1,128]{1,0:T(1,128)} %bitcast.7, bf16[64,1024]{1,0:T(8,128)(2,1)} %bitcast.4, bf16[16,256,128]{2,1,0:T(8,128)(2,1)} %k_hbm.1, ...), custom_call_target="tpu_custom_call" | custom-call | tf_op jit(solution)/shard_map/step/pallas_call | solution.py:381
  53.7 1.3 %copy.12 = bf16[16,32]{1,0:T(8,128)(2,1)} copy(bf16[16,32]{1,0:T(8,128)(2,1)} %step.1) | data formatting | bytes 2048

commit v3 on v2

v3 whole, which is shorter than its diff:
```python
import functools

import jax
import jax.numpy as jnp
import numpy as np
from jax import lax
from jax.experimental import pallas as pl
from jax.experimental.pallas import tpu as pltpu
from jax.sharding import PartitionSpec as P

D = 4096
EPS = 1e-05
NEG = -1e30
N = 8
FAR_FIRST = (4, 3, 5, 2, 6, 1, 7)
OWNERS = 7
MESH = pl.DeviceIdType.MESH
F32 = jnp.float32
BF16 = jnp.bfloat16


def kernel(
    tok_hbm, gain_hbm, wq_hbm, lam_hbm, hgain_hbm, wo_hbm, k_hbm, v_hbm, len_hbm, freq_hbm,
    out_ref,
    tok, gain, wq, lam, hgain, wo, kc, vc, lens, freq,
    qs, sqs, qr, sqr, zs, zsq, zr, zsqr, gs, gr,
    ns, ss, nr, sr, n2s, s2s, n2r, s2r, fs, fr, full,
    local_sem, send_sem, recv_sem, piece_sem,
):
    kv = lax.axis_index("kv")
    tp = lax.axis_index("tp")
    y = lax.rem(kv, N)
    z = lax.div(kv, N)
    last = N - 1

    def load(i, src, dst):
        return pltpu.make_async_copy(src, dst, local_sem.at[i])

    l_tok = load(0, tok_hbm, tok)
    l_gain = load(1, gain_hbm, gain)
    l_wq = load(2, wq_hbm, wq)
    l_wo = load(3, wo_hbm.at[pl.ds(pl.multiple_of(tp * 32, 32), 32), :], wo.at[tp])
    l_len = load(4, len_hbm, lens)
    l_freq = load(5, freq_hbm, freq)
    l_lam = load(6, lam_hbm, lam.at[tp])
    l_hgain = load(7, hgain_hbm, hgain)
    l_k = load(8, k_hbm, kc)
    l_v = load(9, v_hbm, vc)
    for copy in (l_tok, l_gain, l_wq):
        copy.start()

    def at(zp, yp, core):
        return {"kv": zp * N + yp, "tp": core}

    def y_id(d):
        return at(z, lax.rem(y + d, N), 1)

    def z_id(d):
        return at(lax.rem(z + d, N), y, 1)

    def z_id0(d):
        return at(lax.rem(z + d, N), y, 0)

    barrier = pltpu.get_barrier_semaphore()

    def greet(ident):
        pl.semaphore_signal(barrier, inc=1, device_id=ident, device_id_type=MESH)

    @pl.when((tp == 1) & (z < last))
    def _():
        for d in FAR_FIRST:
            greet(z_id(d))
            greet(y_id(d))
        for d in range(N):
            greet(z_id0(d))

    @pl.when((tp == 0) | (z == last))
    def _():
        greet({"tp": 1 - tp})

    @pl.when(tp == 1)
    def _():
        for copy in (l_len, l_freq, l_hgain, l_k, l_v):
            copy.start()

    l_lam.start()
    l_wo.start()

    def copy_to(phase, src, dst, ident):
        return pltpu.make_async_remote_copy(
            src_ref=src, dst_ref=dst, send_sem=send_sem.at[phase], recv_sem=recv_sem.at[phase],
            device_id=ident, device_id_type=MESH,
        )

    def arrived(phase, ref):
        copy_to(phase, ref, ref, z_id0(0)).wait_recv()

    def left(phase, ref):
        copy_to(phase, ref, ref, z_id0(0)).wait_send()

    l_tok.wait()
    l_gain.wait()
    x = tok[...].astype(F32)
    scaled_in = (x * gain[...]).astype(BF16)
    l_wq.wait()
    partial = jnp.dot(scaled_in, wq[...], preferred_element_type=F32)
    for h in range(8):
        qs[pl.ds(h, 16, stride=8), :] = partial[:, 128 * h : 128 * h + 128]
    squares = jnp.broadcast_to(jnp.sum(x * x, -1, keepdims=True), (2 * N, 128))
    for j in range(N):
        sqs[j] = squares[2 * j : 2 * j + 2]

    def rows_of(piece):
        if isinstance(piece, int):
            return pl.ds(piece * 16, 16)
        return pl.ds(pl.multiple_of(piece * 16, 16), 16)

    slot = tp * N + z

    def query_copy(d):
        piece = lax.rem(z + d, OWNERS)
        return copy_to(0, qs.at[rows_of(piece), :], qr.at[0, slot], at(piece, y, 1))

    def square_copy(d):
        piece = lax.rem(z + d, OWNERS)
        return copy_to(2, sqs.at[piece], sqr.at[0, z], at(piece, y, 1))

    def last_query_copy():
        return copy_to(1, qs.at[rows_of(last), :], qr.at[1, slot], at(0, y, 1))

    def last_square_copy():
        return copy_to(3, sqs.at[last], sqr.at[1, z], at(0, y, 1))

    other = {"tp": 1 - tp}
    swap_wo = copy_to(
        4, wo_hbm.at[pl.ds(pl.multiple_of((1 - tp) * 32, 32), 32), :], wo.at[tp], other
    )
    swap_lam = copy_to(5, lam_hbm, lam.at[tp], other)

    @pl.when(tp == 0)
    def _():
        pl.semaphore_wait(barrier, jnp.where(z == last, N, N - 1))

    @pl.when(tp == 1)
    def _():
        pl.semaphore_wait(barrier, jnp.where(z == last, N, 2 * N - 2))

    ORDER = (4, 3, 5, 2, 6, 1)
    for d in ORDER:
        query_copy(d).start()

    @pl.when((tp == 0) | (z == last))
    def _():
        query_copy(0).start()

    @pl.when((tp == 0) | (z > 0))
    def _():
        last_query_copy().start()

    @pl.when(tp == 1)
    def _():
        for d in ORDER:
            square_copy(d).start()

        @pl.when(z == last)
        def _():
            square_copy(0).start()

        @pl.when(z > 0)
        def _():
            last_square_copy().start()

    swap_lam.start()
    swap_wo.start()

    @pl.when(tp == 1)
    def _():
        lane = lax.broadcasted_iota(jnp.int32, (8, 128), 1)
        l_len.wait()
        l_freq.wait()

        def tables_of(piece):
            tables = []
            for b2 in range(2):
                position = (lens[2 * piece + b2] - 1).astype(F32)
                angles = position * jnp.broadcast_to(freq[...], (8, 128))
                tables.append((jnp.cos(angles), jnp.sin(angles)))
            return tables

        def plane_sum(i, piece):
            qr[i, N + z] = qs[rows_of(piece), :]
            sqr[i, z] = sqs[piece]
            arrived(i, qr.at[i, pl.ds(0, 2 * N - 1)])
            arrived(2 + i, sqr.at[i, pl.ds(0, N - 1)])
            for t in range(2):
                zs[i, t] = functools.reduce(lambda a, b: a + b, [qr[i, N * t + k] for k in range(N)])
            zsq[i] = functools.reduce(lambda a, b: a + b, [sqr[i, k] for k in range(N)])
            for d in FAR_FIRST:
                copy_to(6 + i, zs.at[i], zr.at[i, N - d], y_id(d)).start()
                copy_to(8 + i, zsq.at[i], zsqr.at[i, N - d], y_id(d)).start()

        def finished(i, piece, tables):
            arrived(6 + i, zr.at[i, pl.ds(1, N - 1)])
            arrived(8 + i, zsqr.at[i, pl.ds(1, N - 1)])
            total_sq = functools.reduce(lambda a, b: a + b, [zsqr[i, k] for k in range(1, N)], zsq[i])
            scale = lax.rsqrt(total_sq / D + EPS)
            for t in range(2):
                total = functools.reduce(lambda a, b: a + b, [zr[i, k, t] for k in range(1, N)], zs[i, t])
                for b2 in range(2):
                    cosine, sine = tables[b2]
                    q = total[8 * b2 : 8 * b2 + 8] * scale[b2 : b2 + 1]
                    turned = jnp.where((lane & 32) == 0, -pltpu.roll(q, 96, 1), pltpu.roll(q, 32, 1))
                    q = (q * cosine + turned * sine) * 0.125
                    gs[i, t, 8 * b2 : 8 * b2 + 8, :] = q
                    gr[piece, t, 8 * b2 : 8 * b2 + 8, :] = q
            for d in FAR_FIRST:
                pltpu.make_async_remote_copy(
                    src_ref=gs.at[i], dst_ref=gr.at[piece], send_sem=send_sem.at[10 + i],
                    recv_sem=piece_sem.at[piece], device_id=z_id(d), device_id_type=MESH,
                ).start()

        @pl.when((z > 0) & (z < last))
        def _():
            tables = tables_of(z)
            plane_sum(0, z)
            finished(0, z, tables)

        @pl.when(z == 0)
        def _():
            tables = tables_of(0)
            last_tables = tables_of(last)
            plane_sum(0, 0)
            plane_sum(1, last)
            finished(0, 0, tables)
            finished(1, last, last_tables)

        l_k.wait()
        l_v.wait()
        group = lane // 8
        positions = kv * 256 + lax.broadcasted_iota(jnp.int32, (32, 256), 1)

        def attend(d):
            piece = lax.rem(z + d, N)

            @pl.when(((piece != z) | (z == last)) & ((piece != last) | (z != 0)))
            def _():
                pltpu.make_async_remote_copy(
                    src_ref=gs.at[0], dst_ref=gr.at[piece], send_sem=send_sem.at[10],
                    recv_sem=piece_sem.at[piece], device_id=z_id0(0), device_id_type=MESH,
                ).wait_recv()

            stats = jnp.zeros((8, 128), F32)
            for b2 in range(2):
                b = 2 * piece + b2
                q = [gr[piece, t, 8 * b2 : 8 * b2 + 8, :] for t in range(2)]
                rows = jnp.concatenate(
                    [jnp.where(lane < 64, part, 0.0) for part in q]
                    + [jnp.where(lane < 64, 0.0, part) for part in q], 0
                )
                high = rows.astype(BF16)
                low = (rows - high.astype(F32)).astype(BF16)
                scores = lax.dot_general(
                    jnp.concatenate([high, low], 0), kc[b], (((1,), (1,)), ((), ())),
                    preferred_element_type=F32,
                )
                scores = scores[:32] + scores[32:]
                valid = positions < lens[b]
                scores = jnp.where(valid, scores, NEG)
                top = jnp.max(scores, -1, keepdims=True)
                weights = jnp.where(valid, jnp.exp(scores - top), 0.0)
                totals = jnp.sum(weights, -1, keepdims=True)
                numer = jnp.dot(weights.astype(BF16), vc[b], preferred_element_type=F32)
                ns[d, 32 * b2 : 32 * b2 + 32, :] = numer.astype(BF16)
                for i in range(4):
                    k = 4 * b2 + i
                    stats = jnp.where(group == k, top[8 * i : 8 * i + 8], stats)
                    stats = jnp.where(group == 8 + k, totals[8 * i : 8 * i + 8], stats)
            ss[d] = stats
            if d:
                copy_to(12, ss.at[d], sr.at[N - d], z_id(d)).start()
                copy_to(13, ns.at[d], nr.at[N - d], z_id(d)).start()

        for d in (0, 7, 1, 6, 2, 5, 3, 4):
            attend(d)

        def combined(phase, stats, numer, stat_slots, numer_slots):
            arrived(phase, stat_slots.at[pl.ds(1, N - 1)])
            stat = [stats] + [stat_slots[k] for k in range(1, N)]
            top = functools.reduce(jnp.maximum, stat)
            factors = [jnp.exp(s - top) for s in stat]
            total = sum(pltpu.roll(f, 64, 1) * s for f, s in zip(factors, stat))
            arrived(phase + 1, numer_slots.at[pl.ds(1, N - 1)])
            sums = [factors[0][:, 8 * k : 8 * k + 1] * numer[8 * k : 8 * k + 8] for k in range(8)]
            for i in range(1, N):
                block = numer_slots[i].astype(F32)
                for k in range(8):
                    sums[k] = sums[k] + factors[i][:, 8 * k : 8 * k + 1] * block[8 * k : 8 * k + 8]
            return jnp.where(lane < 64, top, total), sums

        stats, sums = combined(12, ss[0], ns[0].astype(F32), sr, nr)
        numer = jnp.concatenate(sums, 0)
        s2s[...] = stats
        n2s[...] = numer.astype(BF16)
        for d in FAR_FIRST:
            copy_to(14, s2s, s2r.at[N - d], y_id(d)).start()
            copy_to(15, n2s, n2r.at[N - d], y_id(d)).start()
        l_hgain.wait()
        l_lam.wait()
        arrived(5, lam.at[0])
        diagonal = lax.broadcasted_iota(jnp.int32, (8, 8), 0) == lax.broadcasted_iota(jnp.int32, (8, 8), 1)
        lambdas = [
            jnp.sum(jnp.where(diagonal, jnp.broadcast_to(lam[t], (8, 8)), 0.0), -1, keepdims=True)
            for t in range(2)
        ]
        stats, sums = combined(14, stats, numer, s2r, n2r)
        normed = []
        for b2 in range(2):
            for t in range(2):
                first, second = (
                    sums[k] / stats[:, 64 + 8 * k : 65 + 8 * k] for k in (4 * b2 + t, 4 * b2 + 2 + t)
                )
                head = first - lambdas[t] * second
                factor = lax.rsqrt(jnp.mean(head * head, -1, keepdims=True) + EPS)
                normed.append(head * factor * hgain[...])
        normed = jnp.concatenate(normed, 0).astype(BF16)
        fs[...] = normed
        for d in FAR_FIRST:
            copy_to(16, fs, fr.at[N - d], z_id0(d)).start()
            copy_to(16, fs, fr.at[N - d], z_id(d)).start()
        copy_to(16, fs, fr.at[0], z_id0(0)).start()
        fr[0] = normed

    @pl.when(tp == 1)
    def _():
        arrived(16, fr.at[pl.ds(1, N - 1)])

    @pl.when(tp == 0)
    def _():
        l_lam.wait()
        arrived(5, lam.at[0])
        arrived(16, fr)

    l_wo.wait()
    arrived(4, wo.at[0])
    for d in range(N):
        full[pl.ds(pl.multiple_of(lax.rem(z + d, N) * 32, 32), 32), :] = fr[d].astype(F32)
    mixed = jnp.zeros((16, 32), F32)
    for t in range(2):
        flat = jnp.concatenate([full[pl.ds(8 * t + h, 16, stride=16), :] for h in range(8)], 1)
        mixed = mixed + lax.dot_general(
            flat.astype(BF16), wo[t], (((1,), (1,)), ((), ())), preferred_element_type=F32
        )
    out_ref[...] = mixed.astype(BF16)

    left(4, wo.at[0])
    left(5, lam.at[0])
    @pl.when((tp == 0) | (z == last))
    def _():
        left(0, qr.at[0, pl.ds(0, OWNERS)])

    @pl.when((tp == 1) & (z < last))
    def _():
        left(0, qr.at[0, pl.ds(0, OWNERS - 1)])

    @pl.when((tp == 0) | (z > 0))
    def _():
        left(1, qr.at[1, 0])

    @pl.when(tp == 1)
    def _():
        @pl.when(z == last)
        def _():
            left(2, sqr.at[0, pl.ds(0, OWNERS)])

        @pl.when(z < last)
        def _():
            left(2, sqr.at[0, pl.ds(0, OWNERS - 1)])
            left(6, zr.at[0, pl.ds(1, N - 1)])
            left(8, zsqr.at[0, pl.ds(1, N - 1)])
            left(10, gr.at[pl.ds(1, N - 1)])

        @pl.when(z > 0)
        def _():
            left(3, sqr.at[1, 0])

        @pl.when(z == 0)
        def _():
            left(7, zr.at[1, pl.ds(1, N - 1)])
            left(9, zsqr.at[1, pl.ds(1, N - 1)])
            left(11, gr.at[pl.ds(1, N - 1)])

        left(12, sr.at[pl.ds(1, N - 1)])
        left(13, nr.at[pl.ds(1, N - 1)])
        left(14, s2r.at[pl.ds(1, N - 1)])
        left(15, n2r.at[pl.ds(1, N - 1)])
        left(16, fr.at[pl.ds(1, N - 1)])
        left(16, fr)


def on_device(tokens, norm_gain, w_query, lambda_head, head_gain, w_out, keys, values, lengths):
    frequency = 1.0 / 10000.0 ** (np.arange(32, dtype=np.float32) / np.float32(32))
    freq = jnp.asarray(np.tile(frequency.astype(np.float32), 4)[None, :])
    operands = (
        tokens, norm_gain[None, :], w_query, lambda_head[None, :], head_gain[None, :], w_out.T, keys, values,
        lengths, freq,
    )
    vmem = pltpu.VMEM
    local = [vmem(a.shape, a.dtype) for a in operands]
    local[3] = vmem((2, 1, 8), F32)
    local[5] = vmem((2, 32, 1024), BF16)
    local[8] = pltpu.SMEM((16,), jnp.int32)
    scratch = local + [
        vmem((128, 128), F32), vmem((N, 2, 128), F32),
        vmem((2, 2 * N, 16, 128), F32), vmem((2, N, 2, 128), F32),
        vmem((2, 2, 16, 128), F32), vmem((2, 2, 128), F32),
        vmem((2, N, 2, 16, 128), F32), vmem((2, N, 2, 128), F32),
        vmem((2, 2, 16, 128), F32), vmem((N, 2, 16, 128), F32),
        vmem((N, 64, 128), BF16), vmem((N, 8, 128), F32), vmem((N, 64, 128), BF16), vmem((N, 8, 128), F32),
        vmem((64, 128), BF16), vmem((8, 128), F32), vmem((N, 64, 128), BF16), vmem((N, 8, 128), F32),
        vmem((32, 128), BF16), vmem((N, 32, 128), BF16), vmem((256, 128), F32),
        pltpu.SemaphoreType.DMA((10,)), pltpu.SemaphoreType.DMA((17,)), pltpu.SemaphoreType.DMA((17,)),
        pltpu.SemaphoreType.DMA((N,)),
    ]
    return pl.pallas_call(
        kernel,
        name="step",
        out_shape=jax.ShapeDtypeStruct((16, 32), BF16),
        in_specs=[pl.BlockSpec(memory_space=pl.ANY)] * len(operands),
        out_specs=pl.BlockSpec(memory_space=pltpu.VMEM),
        scratch_shapes=scratch,
        compiler_params=pltpu.CompilerParams(collective_id=0, has_side_effects=True),
    )(*operands)


def solution(mesh):
    in_specs = (
        P("dp", "kv"),
        P("kv"),
        P("kv", "tp"),
        P("tp"),
        P(),
        P("tp", "kv"),
        P("dp", "kv", None),
        P("dp", "kv", None),
        P("dp"),
    )
    return jax.shard_map(
        on_device, mesh=mesh, in_specs=in_specs, out_specs=P("dp", ("kv", "tp")), check_vma=False
    )
```

time: 55.1 us -> 51.6 us (0.936)
  Pallas kernels: 53.6 us -> 50.1 us
    pallas_call x1, Pallas kernels: 53.6 us -> 50.1 us  [on_device(): pl.pallas_call(kernel, name='step', out_shape=jax.ShapeDtypeStruct((16, 3...]
where the time goes in v3:
time: 51.6 us; the launch traced here: 51.4 us
  Pallas kernels  50.1 us (97%)
  local copies, waits for them, and re-layouts  1.28 us (2%)
    pallas_call x1, Pallas kernels, on_device(): pl.pallas_call(kernel, name='step', out_shape=jax.ShapeDtypeStruct((16, 3...  50.1 us
    unnamed x1, local copies, waits for them, and re-layouts  1.28 us

profile of v3, /device:TPU:1, one launch (start us, length us, event | category | flops | bytes accessed | tf_op | source)
XLA Modules:
  0.0 51.4 jit_solution(3000834286256422122)
XLA Ops:
  0.0 50.1 %step.1 = bf16[16,32]{1,0:T(8,128)(2,1)} custom-call(bf16[16,64]{1,0:T(8,128)(2,1)} %tok_hbm.1, f32[1,64]{1,0:T(1,128)} %bitcast.5, bf16[64,1024]{1,0:T(8,128)(2,1)} %wq_hbm.1, f32[1,8]{1,0:T(1,128)} %bitcast.6, f32[1,128]{1,0:T(1,128)} %bitcast.7, bf16[64,1024]{1,0:T(8,128)(2,1)} %bitcast.4, bf16[16,256,128]{2,1,0:T(8,128)(2,1)} %k_hbm.1, ...), custom_call_target="tpu_custom_call" | custom-call | tf_op jit(solution)/shard_map/step/pallas_call | solution.py:424
  50.1 1.3 %copy.12 = bf16[16,32]{1,0:T(8,128)(2,1)} copy(bf16[16,32]{1,0:T(8,128)(2,1)} %step.1) | data formatting | bytes 2048

commit v4 on v3

--- a/solution.py
+++ b/solution.py
@@ -424,7 +424,7 @@
     return pl.pallas_call(
         kernel,
         name="step",
-        out_shape=jax.ShapeDtypeStruct((16, 32), BF16),
+        out_shape=pltpu.VMEM((16, 32), BF16),
         in_specs=[pl.BlockSpec(memory_space=pl.ANY)] * len(operands),
         out_specs=pl.BlockSpec(memory_space=pltpu.VMEM),
         scratch_shapes=scratch,

time: 51.6 us -> 50.3 us (0.975)
  local copies, waits for them, and re-layouts: 1.28 us -> 0.6 us
  Pallas kernels: 50.1 us -> 49.5 us
    unnamed x1, local copies, waits for them, and re-layouts: 1.28 us -> 0.6 us
    pallas_call x1, Pallas kernels: 50.1 us -> 49.5 us  [on_device(): pl.pallas_call(kernel, name='step', out_shape=pltpu.VMEM((16, 32), BF16),...]
where the time goes in v4:
time: 50.3 us; the launch traced here: 50.2 us
  Pallas kernels  49.5 us (98%)
  local copies, waits for them, and re-layouts  0.6 us (1%)
    pallas_call x1, Pallas kernels, on_device(): pl.pallas_call(kernel, name='step', out_shape=pltpu.VMEM((16, 32), BF16),...  49.5 us

profile of v4, /device:TPU:1, one launch (start us, length us, event | category | flops | bytes accessed | tf_op | source)
XLA Modules:
  0.0 50.2 jit_solution(3455146675202061576)
XLA Ops:
  0.0 49.5 %step.1 = bf16[16,32]{1,0:T(8,128)(2,1)S(1)} custom-call(bf16[16,64]{1,0:T(8,128)(2,1)} %tok_hbm.1, f32[1,64]{1,0:T(1,128)} %bitcast.5, bf16[64,1024]{1,0:T(8,128)(2,1)} %wq_hbm.1, f32[1,8]{1,0:T(1,128)} %bitcast.6, f32[1,128]{1,0:T(1,128)} %bitcast.7, bf16[64,1024]{1,0:T(8,128)(2,1)} %bitcast.4, bf16[16,256,128]{2,1,0:T(8,128)(2,1)} %k_hbm.1, ...), custom_call_target="tpu_custom_call" | custom-call | tf_op jit(solution)/shard_map/step/pallas_call | solution.py:424
  49.6 0.6 %copy.12 = bf16[16,32]{1,0:T(8,128)(2,1)} copy(bf16[16,32]{1,0:T(8,128)(2,1)S(1)} %step.1) | data formatting | bytes 2048

commit v5 on v4

--- a/solution.py
+++ b/solution.py
@@ -237,6 +237,7 @@
         l_k.wait()
         l_v.wait()
         group = lane // 8
+        diagonal = lax.rem(lane, 8) == lax.broadcasted_iota(jnp.int32, (8, 128), 0)
         positions = kv * 256 + lax.broadcasted_iota(jnp.int32, (32, 256), 1)
 
         def attend(d):
@@ -275,27 +276,28 @@
                     k = 4 * b2 + i
                     stats = jnp.where(group == k, top[8 * i : 8 * i + 8], stats)
                     stats = jnp.where(group == 8 + k, totals[8 * i : 8 * i + 8], stats)
-            ss[d] = stats
+            ss[d] = jnp.sum(jnp.where(diagonal, stats, 0.0), 0, keepdims=True)
             if d:
                 copy_to(12, ss.at[d], sr.at[N - d], z_id(d)).start()
                 copy_to(13, ns.at[d], nr.at[N - d], z_id(d)).start()
 
-        for d in (0, 7, 1, 6, 2, 5, 3, 4):
+        for d in (7, 1, 6, 2, 5, 3, 4, 0):
             attend(d)
 
         def combined(phase, stats, numer, stat_slots, numer_slots):
             arrived(phase, stat_slots.at[pl.ds(1, N - 1)])
-            stat = [stats] + [stat_slots[k] for k in range(1, N)]
-            top = functools.reduce(jnp.maximum, stat)
-            factors = [jnp.exp(s - top) for s in stat]
-            total = sum(pltpu.roll(f, 64, 1) * s for f, s in zip(factors, stat))
+            stat = jnp.concatenate([stats] + [stat_slots[k] for k in range(1, N)], 0)
+            top = jnp.max(stat, 0, keepdims=True)
+            factors = jnp.exp(stat - top)
+            total = jnp.sum(pltpu.roll(factors, 64, 1) * stat, 0, keepdims=True)
+            columns = factors.T
             arrived(phase + 1, numer_slots.at[pl.ds(1, N - 1)])
-            sums = [factors[0][:, 8 * k : 8 * k + 1] * numer[8 * k : 8 * k + 8] for k in range(8)]
+            sums = [columns[8 * k : 8 * k + 8, :1] * numer[8 * k : 8 * k + 8] for k in range(8)]
             for i in range(1, N):
                 block = numer_slots[i].astype(F32)
                 for k in range(8):
-                    sums[k] = sums[k] + factors[i][:, 8 * k : 8 * k + 1] * block[8 * k : 8 * k + 8]
-            return jnp.where(lane < 64, top, total), sums
+                    sums[k] = sums[k] + columns[8 * k : 8 * k + 8, i : i + 1] * block[8 * k : 8 * k + 8]
+            return jnp.where(lane[:1] < 64, top, total), sums
 
         stats, sums = combined(12, ss[0], ns[0].astype(F32), sr, nr)
         numer = jnp.concatenate(sums, 0)
@@ -307,17 +309,17 @@
         l_hgain.wait()
         l_lam.wait()
         arrived(5, lam.at[0])
-        diagonal = lax.broadcasted_iota(jnp.int32, (8, 8), 0) == lax.broadcasted_iota(jnp.int32, (8, 8), 1)
         lambdas = [
-            jnp.sum(jnp.where(diagonal, jnp.broadcast_to(lam[t], (8, 8)), 0.0), -1, keepdims=True)
+            jnp.sum(jnp.where(diagonal[:, :8], jnp.broadcast_to(lam[t], (8, 8)), 0.0), -1, keepdims=True)
             for t in range(2)
         ]
         stats, sums = combined(14, stats, numer, s2r, n2r)
+        totals = jnp.broadcast_to(stats, (8, 128)).T
         normed = []
         for b2 in range(2):
             for t in range(2):
                 first, second = (
-                    sums[k] / stats[:, 64 + 8 * k : 65 + 8 * k] for k in (4 * b2 + t, 4 * b2 + 2 + t)
+                    sums[k] / totals[64 + 8 * k : 72 + 8 * k, :1] for k in (4 * b2 + t, 4 * b2 + 2 + t)
                 )
                 head = first - lambdas[t] * second
                 factor = lax.rsqrt(jnp.mean(head * head, -1, keepdims=True) + EPS)
@@ -415,8 +417,8 @@
         vmem((2, 2, 16, 128), F32), vmem((2, 2, 128), F32),
         vmem((2, N, 2, 16, 128), F32), vmem((2, N, 2, 128), F32),
         vmem((2, 2, 16, 128), F32), vmem((N, 2, 16, 128), F32),
-        vmem((N, 64, 128), BF16), vmem((N, 8, 128), F32), vmem((N, 64, 128), BF16), vmem((N, 8, 128), F32),
-        vmem((64, 128), BF16), vmem((8, 128), F32), vmem((N, 64, 128), BF16), vmem((N, 8, 128), F32),
+        vmem((N, 64, 128), BF16), vmem((N, 1, 128), F32), vmem((N, 64, 128), BF16), vmem((N, 1, 128), F32),
+        vmem((64, 128), BF16), vmem((1, 128), F32), vmem((N, 64, 128), BF16), vmem((N, 1, 128), F32),
         vmem((32, 128), BF16), vmem((N, 32, 128), BF16), vmem((256, 128), F32),
         pltpu.SemaphoreType.DMA((10,)), pltpu.SemaphoreType.DMA((17,)), pltpu.SemaphoreType.DMA((17,)),
         pltpu.SemaphoreType.DMA((N,)),

time: 50.3 us -> 48.9 us (0.972)
  Pallas kernels: 49.5 us -> 48.1 us
    pallas_call x1, Pallas kernels: 49.5 us -> 48.1 us  [on_device(): pl.pallas_call(kernel, name='step', out_shape=pltpu.VMEM((16, 32), BF16),...]
where the time goes in v5:
time: 48.9 us; the launch traced here: 48.7 us
  Pallas kernels  48.1 us (98%)
  local copies, waits for them, and re-layouts  0.6 us (1%)
    pallas_call x1, Pallas kernels, on_device(): pl.pallas_call(kernel, name='step', out_shape=pltpu.VMEM((16, 32), BF16),...  48.1 us

profile of v5, /device:TPU:1, one launch (start us, length us, event | category | flops | bytes accessed | tf_op | source)
XLA Modules:
  0.0 48.7 jit_solution(16003606476404590704)
XLA Ops:
  0.0 48.1 %step.1 = bf16[16,32]{1,0:T(8,128)(2,1)S(1)} custom-call(bf16[16,64]{1,0:T(8,128)(2,1)} %tok_hbm.1, f32[1,64]{1,0:T(1,128)} %bitcast.5, bf16[64,1024]{1,0:T(8,128)(2,1)} %wq_hbm.1, f32[1,8]{1,0:T(1,128)} %bitcast.6, f32[1,128]{1,0:T(1,128)} %bitcast.7, bf16[64,1024]{1,0:T(8,128)(2,1)} %bitcast.4, bf16[16,256,128]{2,1,0:T(8,128)(2,1)} %k_hbm.1, ...), custom_call_target="tpu_custom_call" | custom-call | tf_op jit(solution)/shard_map/step/pallas_call | solution.py:426
  48.2 0.6 %copy.12 = bf16[16,32]{1,0:T(8,128)(2,1)} copy(bf16[16,32]{1,0:T(8,128)(2,1)S(1)} %step.1) | data formatting | bytes 2048

commit v6 on v5

--- a/solution.py
+++ b/solution.py
@@ -281,7 +281,7 @@
                 copy_to(12, ss.at[d], sr.at[N - d], z_id(d)).start()
                 copy_to(13, ns.at[d], nr.at[N - d], z_id(d)).start()
 
-        for d in (7, 1, 6, 2, 5, 3, 4, 0):
+        for d in (7, 1, 6, 2, 5, 4, 3, 0):
             attend(d)
 
         def combined(phase, stats, numer, stat_slots, numer_slots):

time: 48.9 us -> 48.7 us (level)
  no operation moved by 1% of the time
where the time goes in v6:
time: 48.7 us; the launch traced here: 48.6 us
  Pallas kernels  48 us (99%)
  local copies, waits for them, and re-layouts  0.6 us (1%)
    pallas_call x1, Pallas kernels, on_device(): pl.pallas_call(kernel, name='step', out_shape=pltpu.VMEM((16, 32), BF16),...  48 us

profile of v6, /device:TPU:1, one launch (start us, length us, event | category | flops | bytes accessed | tf_op | source)
XLA Modules:
  0.0 48.6 jit_solution(5348377304012696292)
XLA Ops:
  0.0 48.0 %step.1 = bf16[16,32]{1,0:T(8,128)(2,1)S(1)} custom-call(bf16[16,64]{1,0:T(8,128)(2,1)} %tok_hbm.1, f32[1,64]{1,0:T(1,128)} %bitcast.5, bf16[64,1024]{1,0:T(8,128)(2,1)} %wq_hbm.1, f32[1,8]{1,0:T(1,128)} %bitcast.6, f32[1,128]{1,0:T(1,128)} %bitcast.7, bf16[64,1024]{1,0:T(8,128)(2,1)} %bitcast.4, bf16[16,256,128]{2,1,0:T(8,128)(2,1)} %k_hbm.1, ...), custom_call_target="tpu_custom_call" | custom-call | tf_op jit(solution)/shard_map/step/pallas_call | solution.py:426
  48.0 0.6 %copy.12 = bf16[16,32]{1,0:T(8,128)(2,1)} copy(bf16[16,32]{1,0:T(8,128)(2,1)S(1)} %step.1) | data formatting | bytes 2048
